TPU v7x, 256 devices: a whole 4x4x8 slice. The times are simulated.
256 devices in a mesh: ep: 64 (over z, x, core), tp: 4 (over y).
Axes of the slice: x: 4, y: 4, z: 8, core: 2. Of those that a mesh axis runs over, the one named last changes fastest.
Arguments:
- queries: bfloat16 [32768, 1024], P('ep', 'tp'), may hold values from -6 to 6
- forget_forward_logits: bfloat16 [32768, 1024], P('ep', 'tp'), may hold values from -6 to 12
- forget_backward_logits: bfloat16 [32768, 1024], P('ep', 'tp'), may hold values from -6 to 12
- values: bfloat16 [32768, 1024], P('ep', 'tp'), may hold values from -6 to 6
- output_gate_logits: bfloat16 [32768, 1024], P('ep', 'tp'), may hold values from -6 to 6
- lower_bound_forward: float32 [1024], P('tp')
- lower_bound_backward: float32 [1024], P('tp')
- extra_log_decay: float32 [32768, 8], P('ep', 'tp'), may hold values from -2 to 0
- head_norm_scale: float32 [1024], P('tp'), may hold values from 0.1 to 1.9
- output_projection: bfloat16 [1024, 2048], P('tp'), may hold values from -0.1875 to 0.1875
- second_residual: bfloat16 [32768, 2048], P('ep'), may hold values from -6 to 6
- expert_norm_scale: float32 [2048], replicated, may hold values from 0.1 to 1.9
- routes: int32 [32768, 2], P('ep'), may hold values from 0 to 63, all different within a row; in each aligned block of 128 rows (0 to 127, 128 to 255, ...) at most 8 rows name the same one
- specialist_mixing_factor: float32 [32768, 2], P(('ep', 'tp')), may hold values from 0.1 to 1
- expert_gate_matrix: bfloat16 [64, 2048, 1024], P('ep', None, 'tp'), may hold values from -0.125 to 0.125
- expert_up_matrix: bfloat16 [64, 2048, 1024], P('ep', None, 'tp'), may hold values from -0.125 to 0.125
- expert_down_matrix: bfloat16 [64, 1024, 2048], P('ep', 'tp'), may hold values from -0.1875 to 0.1875
Outputs:
- mixer_output: bfloat16 [32768, 2048], P(('ep', 'tp'))
- routed_output: bfloat16 [32768, 2048], P(('ep', 'tp'))
Inputs may be any that keep to these rules, and one draw needn't show every extreme that they name: `routes`: in each aligned block of 128 rows no expert is named by more than 8 rows; the 2 experts of a row differ.
All inputs are finite; a program needn't handle non-finite values.
Results may differ from a plain program's by a relative error of at most 0.014.
Values may be sent and summed in bfloat16 or wider, within the bound.
A program may use at most 128 MiB of HBM per device.

v0:
```python
import jax
import jax.numpy as jnp
from jax import lax
from jax.sharding import Mesh
from jax.sharding import PartitionSpec as P

TOPK = 2
SPAN = 64
EP = ("ep_0", "ep_1", "ep_2")
EP_TP = ("ep_0", "ep_1", "ep_2", "tp")


EPS = 1e-06


def filled_with(shard, identity):
    return jax.tree.map(
        lambda a, e: jnp.broadcast_to(jnp.asarray(e, a.dtype), a.shape), shard, identity
    )


def entering(shard, axes, combine, identity, reverse):
    before = start = filled_with(shard, identity)
    so_far = shard
    for axis in reversed(axes):
        size, index = (lax.axis_size(axis), lax.axis_index(axis))
        pieces = jax.tree.map(
            lambda part, kind: lax.all_gather(part.astype(kind), axis),
            so_far,
            (jnp.bfloat16, jnp.bfloat16),
        )
        inside, so_far = (start, start)
        for k in reversed(range(size)) if reverse else range(size):
            passed = k > index if reverse else k < index
            so_far = combine(
                so_far, jax.tree.map(lambda part, own: part[k].astype(own.dtype), pieces, shard)
            )
            inside = jax.tree.map(lambda new, old: jnp.where(passed, new, old), so_far, inside)
        before = combine(inside, before)
    return before


def laid_out(pieces, dim):
    pieces = jnp.moveaxis(pieces, 0, dim)
    dims = pieces.shape
    return pieces.reshape(*dims[:dim], dims[dim] * dims[dim + 1], *dims[dim + 2 :])


def work_in_pieces(shard, axis, dim, apply, out_dim):
    size, span = (lax.axis_size(axis), shard.shape[dim])
    count = 2 if span % 2 == 0 else 1
    outs, length = ([], span // count)
    for k in range(count):
        share = lax.slice_in_dim(shard, k * length, (k + 1) * length, axis=dim)
        starts = jnp.arange(size) * span + k * length
        outs.append(jax.vmap(apply)(lax.all_gather(share, axis), starts))
    return laid_out(jnp.concatenate(outs, axis=out_dim + 1), out_dim)


def block_pass(feature, key_matrix_rows, value_rows, log_forget_decay):
    row_count, number_of_heads, channels = feature.shape
    blocks = row_count // SPAN
    lower_mask = jnp.tril(jnp.ones((SPAN, SPAN), bool))[:, :, None, None]

    def shaped(tensor):
        return tensor.reshape(blocks, SPAN, number_of_heads, tensor.shape[-1])

    def advance(progress, inputs):
        recurrent_memory, offset = progress
        query_tile_rows, address_piece_entries, content_piece_entries, decay_block = inputs
        progressive_summary = jnp.cumsum(decay_block, axis=0)
        spread_log = jnp.where(
            lower_mask, progressive_summary[:, None] - progressive_summary[None, :], -jnp.inf
        )
        scores = jnp.sum(
            query_tile_rows[:, None] * address_piece_entries[None, :] * jnp.exp(spread_log), axis=-1
        )
        inner_part = jnp.einsum("tsh,shv->thv", scores, content_piece_entries)
        handed_summary = jnp.einsum(
            "wbf,bfl->wbl", query_tile_rows * jnp.exp(progressive_summary), recurrent_memory
        )
        segment_fading_total = progressive_summary[-1]
        trained_portion = jnp.einsum(
            "gkf,gkr->kfr",
            address_piece_entries * jnp.exp(segment_fading_total[None] - progressive_summary),
            content_piece_entries,
        )
        recurrent_memory = (
            jnp.exp(segment_fading_total)[:, :, None] * recurrent_memory + trained_portion
        )
        return (
            (recurrent_memory, offset + segment_fading_total),
            (inner_part + handed_summary, query_tile_rows * jnp.exp(progressive_summary + offset)),
        )

    initial = (
        jnp.zeros((number_of_heads, channels, value_rows.shape[-1]), jnp.float32),
        jnp.zeros((number_of_heads, channels), jnp.float32),
    )
    (recurrent_memory, decay_total), (output_rows, query_decay_reach) = lax.scan(
        advance,
        initial,
        (shaped(feature), shaped(key_matrix_rows), shaped(value_rows), shaped(log_forget_decay)),
    )
    return (
        output_rows.reshape(row_count, number_of_heads, -1),
        query_decay_reach.reshape(row_count, number_of_heads, channels),
        recurrent_memory,
        decay_total,
    )


def forget_gate_terms(forget_gate_input, lower_bound_logit, extra_decay_rows, number_of_heads):
    row_count = forget_gate_input.shape[0]
    widened_values = forget_gate_input.astype(jnp.float32).reshape(row_count, number_of_heads, -1)
    lower_bound_share = jax.nn.sigmoid(lower_bound_logit).reshape(number_of_heads, -1)
    remaining_fraction = jax.nn.sigmoid(-lower_bound_logit).reshape(number_of_heads, -1)
    log_forget_decay = (
        jnp.log(lower_bound_share + remaining_fraction * jax.nn.sigmoid(widened_values))
        + extra_decay_rows[:, :, None]
    )
    return (remaining_fraction * jax.nn.sigmoid(-widened_values), log_forget_decay)


def finish_heads(combined, head_norm_scale, output_gate_logits, number_of_heads):
    mean_square = jnp.mean(combined * combined, axis=-1, keepdims=True)
    scaled = combined * lax.rsqrt(mean_square + EPS) * head_norm_scale.reshape(number_of_heads, -1)
    opened = scaled * jax.nn.silu(output_gate_logits.astype(jnp.float32)).reshape(combined.shape)
    return opened.astype(jnp.bfloat16).reshape(combined.shape[0], -1)


def normalize(tensor, gain):
    widened_values = tensor.astype(jnp.float32)
    return (
        widened_values
        * lax.rsqrt(jnp.mean(widened_values * widened_values, axis=-1, keepdims=True) + EPS)
        * gain
    ).astype(jnp.bfloat16)


def link_states(earlier, later_part):
    decay_early, memory_early = earlier
    decay_late, memory_late = later_part
    return (decay_early + decay_late, jnp.exp(decay_late)[:, :, None] * memory_early + memory_late)


def recurrent_half(
    queries,
    forget_forward_logits,
    forget_backward_logits,
    values,
    output_gate_logits,
    lower_bound_forward,
    lower_bound_backward,
    extra_log_decay,
    head_norm_scale,
    output_projection,
):
    row_count = queries.shape[0]
    number_of_heads = extra_log_decay.shape[1]
    feature = jax.nn.silu(queries.astype(jnp.float32)).reshape(row_count, number_of_heads, -1)
    value_rows = values.astype(jnp.float32).reshape(row_count, number_of_heads, -1)
    combined = jnp.zeros(value_rows.shape, jnp.float32)
    for forget_gate_input, lower_bound_logit, reverse in (
        (forget_forward_logits, lower_bound_forward, False),
        (forget_backward_logits, lower_bound_backward, True),
    ):
        key_matrix_rows, log_forget_decay = forget_gate_terms(
            forget_gate_input, lower_bound_logit, extra_log_decay, number_of_heads
        )
        if reverse:
            output_rows, query_decay_reach, recurrent_memory, decay_total = block_pass(
                jnp.flip(feature, 0),
                jnp.flip(key_matrix_rows, 0),
                jnp.flip(value_rows, 0),
                jnp.flip(log_forget_decay, 0),
            )
        else:
            output_rows, query_decay_reach, recurrent_memory, decay_total = block_pass(
                feature, key_matrix_rows, value_rows, log_forget_decay
            )
        identity = (jnp.zeros_like(decay_total), jnp.zeros_like(recurrent_memory))
        incoming_rows = entering(
            (decay_total, recurrent_memory), EP, link_states, identity, reverse
        )
        output_rows = output_rows + jnp.einsum("wbf,bfl->wbl", query_decay_reach, incoming_rows[1])
        if reverse:
            output_rows = jnp.flip(output_rows, 0)
        combined = combined + output_rows
    mixer_hidden = finish_heads(combined, head_norm_scale, output_gate_logits, number_of_heads)
    return lax.psum_scatter(
        jnp.dot(mixer_hidden, output_projection, preferred_element_type=jnp.float32).astype(
            jnp.bfloat16
        ),
        "tp",
        scatter_dimension=0,
        tiled=True,
    )


def expert_hidden(rows_in, expert_gate_matrix, expert_up_matrix):
    gated = jnp.dot(rows_in, expert_gate_matrix[0], preferred_element_type=jnp.float32)
    lifted = jnp.dot(rows_in, expert_up_matrix[0], preferred_element_type=jnp.float32)
    return (jax.nn.silu(gated) * lifted).astype(jnp.bfloat16)


def routed_half(
    second_residual,
    expert_norm_scale,
    routes,
    specialist_mixing_factor,
    expert_gate_matrix,
    expert_up_matrix,
    expert_down_matrix,
):
    group_rows, width_model = second_residual.shape
    quarters = lax.axis_size("tp")
    experts = lax.axis_size(EP)
    row_count = group_rows // quarters
    slot_count = 2 * TOPK * row_count // experts
    quarter = lax.axis_index("tp")
    own_rows = normalize(
        lax.dynamic_slice_in_dim(second_residual, quarter * row_count, row_count, 0),
        expert_norm_scale,
    )
    flat_routes = lax.dynamic_slice_in_dim(routes, quarter * row_count, row_count, 0).reshape(-1)
    expert_hits = (flat_routes[:, None] == jnp.arange(experts, dtype=jnp.int32)[None, :]).astype(
        jnp.int32
    )
    ranking = jnp.sum(jnp.cumsum(expert_hits, axis=0) * expert_hits, axis=1) - 1
    target = flat_routes * slot_count + ranking
    own_pick = (
        target[:, None] == jnp.arange(experts * slot_count, dtype=jnp.int32)[None, :]
    ).astype(jnp.bfloat16)
    chooser = own_pick.reshape(row_count, TOPK, -1).sum(axis=1)
    outgoing = jnp.einsum(
        "rs,rd->sd", chooser, own_rows, preferred_element_type=jnp.float32
    ).astype(jnp.bfloat16)
    arrived = lax.all_to_all(
        outgoing.reshape(experts, slot_count, width_model),
        EP,
        split_axis=0,
        concat_axis=0,
        tiled=True,
    )

    def lift_rows(fragment, first_row):
        return expert_hidden(fragment, expert_gate_matrix, expert_up_matrix)

    hidden = work_in_pieces(arrived.reshape(-1, width_model), "tp", 0, lift_rows, 0)
    summed = lax.psum_scatter(
        jnp.dot(hidden, expert_down_matrix[0], preferred_element_type=jnp.float32).astype(
            jnp.bfloat16
        ),
        "tp",
        scatter_dimension=0,
        tiled=True,
    )
    returned = lax.all_to_all(
        summed.reshape(experts, slot_count, width_model),
        EP,
        split_axis=0,
        concat_axis=0,
        tiled=True,
    )
    gathered = jnp.dot(
        own_pick, returned.reshape(-1, width_model), preferred_element_type=jnp.float32
    )
    blended = jnp.sum(
        gathered.reshape(row_count, TOPK, width_model) * specialist_mixing_factor[:, :, None],
        axis=1,
    )
    return blended.astype(jnp.bfloat16)


def shards(
    queries,
    forget_forward_logits,
    forget_backward_logits,
    values,
    output_gate_logits,
    lower_bound_forward,
    lower_bound_backward,
    extra_log_decay,
    head_norm_scale,
    output_projection,
    second_residual,
    expert_norm_scale,
    routes,
    specialist_mixing_factor,
    expert_gate_matrix,
    expert_up_matrix,
    expert_down_matrix,
):
    mixer_output = recurrent_half(
        queries,
        forget_forward_logits,
        forget_backward_logits,
        values,
        output_gate_logits,
        lower_bound_forward,
        lower_bound_backward,
        extra_log_decay,
        head_norm_scale,
        output_projection,
    )
    routed_output = routed_half(
        second_residual,
        expert_norm_scale,
        routes,
        specialist_mixing_factor,
        expert_gate_matrix,
        expert_up_matrix,
        expert_down_matrix,
    )
    return (mixer_output, routed_output)


def solution(mesh):
    split = Mesh(mesh.devices.reshape(8, 4, 2, mesh.shape["tp"]), ("ep_0", "ep_1", "ep_2", "tp"))
    return jax.shard_map(
        shards,
        mesh=split,
        in_specs=(
            P(EP, "tp"),
            P(EP, "tp"),
            P(EP, "tp"),
            P(EP, "tp"),
            P(EP, "tp"),
            P("tp"),
            P("tp"),
            P(EP, "tp"),
            P("tp"),
            P("tp", None),
            P(EP, None),
            P(),
            P(EP, None),
            P(EP_TP, None),
            P(EP, None, "tp"),
            P(EP, None, "tp"),
            P(EP, "tp", None),
        ),
        out_specs=(P(EP_TP, None), P(EP_TP, None)),
        check_vma=False,
    )
```

profile of v0, /device:TPU:1, one launch (start us, length us, event | category | flops | bytes accessed | tf_op | source)
XLA Modules:
  0.0 439.2 jit_solution(3195071865625589148)
XLA Ops:
  11.6 1.9 fusion.56
  13.5 62.6 %all_to_all.10 = bf16[64,8,2048]{2,1,0:T(8,128)(2,1)S(1)} all-to-all(bf16[64,8,2048]{2,1,0:T(8,128)(2,1)S(1)} %fusion.56), channel_id=1, replica_groups=mesh['ep_0'=8,'ep_1'=4,'ep_2'=2,'tp'=4] {'ep_0','ep_1','ep_2'}, dimensions={0} | all-to-all | bytes 4194304 | tf_op jit(solution)/shard_map/all_to_all | solution.py:239
  76.1 1.5 slice_bitcast_fusion.3
  81.5 2.5 broadcast_multiply_fusion.1
  85.1 53.0 %while.34 = (s32[]{:T(128)}, f32[2,128,128]{2,1,0:T(8,128)S(1)}, f32[2,128]{1,0:T(2,128)S(1)}, f32[8,64,2,128]{3,1,0,2:T(8,128)S(1)}, bf16[8,64,2,128]{3,2,1,0:T...) while((s32[]{:T(128)}, f32[2,128,128]{2,1,0:T(8,128)S(1)}, ...), condition=%wide.region_3.4_spmd.clone, body=%wide.region_0.3_spmd.clone.sunk | while | flops 17019396 | bytes 2019457 | solution.py:100
  87.1 2.0 multiply_reduce_fusion.5
  93.7 2.0 multiply_reduce_fusion.5
  100.3 2.0 multiply_reduce_fusion.5
  106.9 2.0 multiply_reduce_fusion.5
  113.6 2.0 multiply_reduce_fusion.5
  120.2 2.0 multiply_reduce_fusion.5
  126.8 2.0 multiply_reduce_fusion.5
  133.4 2.0 multiply_reduce_fusion.5
  138.5 2.0 fusion.88
  140.5 2.1 div.74
  143.7 2.5 broadcast_multiply_fusion
  146.3 2.0 rev.16
  150.5 4.8 %fusion.74 = f32[4,256,256]{2,1,0:T(8,128)} fusion(bf16[4,256,2048]{2,1,0:T(8,128)(2,1)} %all-gather.9.cloned.1.call-done, bf16[1,2048,256]{2,1,0:T(8,128)(2,1)} %param.35), kind=kOutput, calls=%fused_computation.107 | convolution fusion | flops 1073741824 | bytes 6291456 | tf_op jit(solution)/shard_map/vmap()/dot_general | solution.py:202
  155.2 24.0 %all-gather.11.cloned.1.call-done = bf16[4,256,2048]{2,1,0:T(8,128)(2,1)} async-done(((bf16[1,256,2048]{2,1,0:T(8,128)(2,1)}), bf16[4,256,2048]{2,1,0:T(8,128)(2,1)}) %all-gather.11.cloned.1.call-update) | async-done | bytes 4194320 | tf_op jit(solution)/shard_map/all_gather | solution.py:56
  179.2 3.9 fusion.72
  187.1 5.6 %convolution_convert_fusion = bf16[2048,2048]{1,0:T(8,128)(2,1)} fusion(bf16[2048,256]{1,0:T(8,128)(2,1)S(1)} %bitcast.557, bf16[1,256,2048]{2,1,0:T(8,128)(2,1)S(1)} %copy-done), kind=kOutput, calls=%fused_computation.78 | convolution fusion | flops 2151677952 | bytes 10485760 | tf_op jit(solution)/shard_map/dot_general | solution.py:252
  193.6 40.7 %while.35 = (s32[]{:T(128)}, f32[2,128,128]{2,1,0:T(8,128)S(1)}, f32[2,128]{1,0:T(2,128)S(1)}, f32[8,64,2,128]{3,1,0,2:T(8,128)S(1)}, bf16[8,64,2,128]{3,2,1,0:T...) while((s32[]{:T(128)}, f32[2,128,128]{2,1,0:T(8,128)S(1)}, ...), condition=%wide.region_7.8_spmd.clone, body=%wide.region_4.7_spmd.clone.sunk | while | flops 17019396 | bytes 2034825 | solution.py:100
  195.6 2.0 multiply_reduce_fusion.6
  200.6 2.0 multiply_reduce_fusion.6
  205.8 2.0 multiply_reduce_fusion.6
  210.8 2.0 multiply_reduce_fusion.6
  215.9 2.0 multiply_reduce_fusion.6
  221.0 2.0 multiply_reduce_fusion.6
  226.1 2.0 multiply_reduce_fusion.6
  231.2 2.0 multiply_reduce_fusion.6
  234.5 2.3 all-gather.5
  236.9 8.4 %all_gather.78 = bf16[4,2,128]{2,1,0:T(2,128)(2,1)S(1)} all-gather(bf16[1,2,128]{2,1,0:T(2,128)(2,1)S(1)} %get-tuple-element.387), channel_id=1, replica_groups=mesh['ep_0'=8,'ep_1'=4,'ep_2'=2,'tp'=4] {'ep_1'}, dimensions={0}, use_global_device_ids=true | all-gather | bytes 2560 | tf_op jit(solution)/shard_map/all_gather | solution.py:28
  245.3 14.4 %all_gather.79 = bf16[8,2,128]{2,1,0:T(2,128)(2,1)S(1)} all-gather(bf16[1,2,128]{2,1,0:T(2,128)(2,1)S(1)} %get-tuple-element.375), channel_id=1, replica_groups=mesh['ep_0'=8,'ep_1'=4,'ep_2'=2,'tp'=4] {'ep_0'}, dimensions={0}, use_global_device_ids=true | all-gather | bytes 4608 | tf_op jit(solution)/shard_map/all_gather | solution.py:28
  259.8 5.3 %all-gather.3 = bf16[4,128,128]{2,1,0:T(8,128)(2,1)S(1)} all-gather(bf16[2,128,128]{2,1,0:T(8,128)(2,1)S(1)} %convert_element_type.660), channel_id=5, replica_groups=mesh['ep_0'=8,'ep_1'=4,'ep_2'=2,'tp'=4] {'ep_2'}, dimensions={0}, use_global_device_ids=true | all-gather | bytes 196608 | tf_op jit(solution)/shard_map/all_gather | solution.py:28
  265.2 10.4 %all_gather.82 = bf16[4,2,128,128]{3,2,1,0:T(8,128)(2,1)S(1)} all-gather(bf16[1,2,128,128]{3,2,1,0:T(8,128)(2,1)S(1)} %fusion.158), channel_id=1, replica_groups=mesh['ep_0'=8,'ep_1'=4,'ep_2'=2,'tp'=4] {'ep_1'}, dimensions={0}, use_global_device_ids=true | all-gather | bytes 327680 | tf_op jit(solution)/shard_map/all_gather | solution.py:28
  275.8 20.0 %all_gather.83 = bf16[8,2,128,128]{3,2,1,0:T(8,128)(2,1)S(1)} all-gather(bf16[1,2,128,128]{3,2,1,0:T(8,128)(2,1)S(1)} %fusion.148), channel_id=1, replica_groups=mesh['ep_0'=8,'ep_1'=4,'ep_2'=2,'tp'=4] {'ep_0'}, dimensions={0}, use_global_device_ids=true | all-gather | bytes 589824 | tf_op jit(solution)/shard_map/all_gather | solution.py:28
  295.8 2.2 fusion.65
  301.1 9.2 %all-gather.4 = bf16[2,2,128]{2,1,0:T(2,128)(2,1)S(1)} all-gather(bf16[1,2,128]{2,1,0:T(2,128)(2,1)S(1)} %convert_bitcast_fusion.13), channel_id=2, replica_groups=mesh['ep_0'=8,'ep_1'=4,'ep_2'=2,'tp'=4] {'ep_2'}, dimensions={0}, use_global_device_ids=true | all-gather | bytes 1536 | tf_op jit(solution)/shard_map/all_gather | solution.py:28
  310.3 5.2 %all_gather.70 = bf16[4,2,128]{2,1,0:T(2,128)(2,1)S(1)} all-gather(bf16[1,2,128]{2,1,0:T(2,128)(2,1)S(1)} %get-tuple-element.379), channel_id=1, replica_groups=mesh['ep_0'=8,'ep_1'=4,'ep_2'=2,'tp'=4] {'ep_1'}, dimensions={0}, use_global_device_ids=true | all-gather | bytes 2560 | tf_op jit(solution)/shard_map/all_gather | solution.py:28
  315.6 10.5 %all_gather.71 = bf16[8,2,128]{2,1,0:T(2,128)(2,1)S(1)} all-gather(bf16[1,2,128]{2,1,0:T(2,128)(2,1)S(1)} %get-tuple-element.370), channel_id=1, replica_groups=mesh['ep_0'=8,'ep_1'=4,'ep_2'=2,'tp'=4] {'ep_0'}, dimensions={0}, use_global_device_ids=true | all-gather | bytes 4608 | tf_op jit(solution)/shard_map/all_gather | solution.py:28
  326.1 7.4 %all-gather.1 = bf16[4,128,128]{2,1,0:T(8,128)(2,1)S(1)} all-gather(bf16[2,128,128]{2,1,0:T(8,128)(2,1)S(1)} %convert_element_type.605), channel_id=3, replica_groups=mesh['ep_0'=8,'ep_1'=4,'ep_2'=2,'tp'=4] {'ep_2'}, dimensions={0}, use_global_device_ids=true | all-gather | bytes 196608 | tf_op jit(solution)/shard_map/all_gather | solution.py:28
  333.6 9.4 %all_gather.74 = bf16[4,2,128,128]{3,2,1,0:T(8,128)(2,1)S(1)} all-gather(bf16[1,2,128,128]{3,2,1,0:T(8,128)(2,1)S(1)} %fusion.154), channel_id=1, replica_groups=mesh['ep_0'=8,'ep_1'=4,'ep_2'=2,'tp'=4] {'ep_1'}, dimensions={0}, use_global_device_ids=true | all-gather | bytes 327680 | tf_op jit(solution)/shard_map/all_gather | solution.py:28
  343.2 19.7 %all_gather.75 = bf16[8,2,128,128]{3,2,1,0:T(8,128)(2,1)S(1)} all-gather(bf16[1,2,128,128]{3,2,1,0:T(8,128)(2,1)S(1)} %fusion.130), channel_id=1, replica_groups=mesh['ep_0'=8,'ep_1'=4,'ep_2'=2,'tp'=4] {'ep_0'}, dimensions={0}, use_global_device_ids=true | all-gather | bytes 589824 | tf_op jit(solution)/shard_map/all_gather | solution.py:28
  363.0 2.2 multiply_reduce_fusion.2
  365.3 16.1 %all-to-all-start.1 = ((bf16[64,8,2048]{2,1,0:T(8,128)(2,1)}), bf16[64,8,2048]{2,1,0:T(8,128)(2,1)S(1)}, u32[]{:S(2)}, u32[]{:S(2)}) async-start(bf16[64,8,2048]{2,1,0:T(8,128)(2,1)} %bitcast.561), calls=%async_computation.3 | async-start | bytes 4194304 | tf_op jit(solution)/shard_map/all_to_all | solution.py:259
  381.4 3.3 convolution_convert_fusion.2
  384.8 46.3 %all-to-all-done.1 = bf16[64,8,2048]{2,1,0:T(8,128)(2,1)S(1)} async-done(((bf16[64,8,2048]{2,1,0:T(8,128)(2,1)}), bf16[64,8,2048]{2,1,0:T(8,128)(2,1)S(1)}, u32[]{:S(2)}, u32[]{:S(2)}) %all-to-all-start.1) | async-done | bytes 2097184 | tf_op jit(solution)/shard_map/all_to_all | solution.py:259
  431.1 1.6 fusion.58
  (283 shorter events, 83.3 us)
Async XLA Ops:
  7.2 180.0 %copy-start = (bf16[1,256,2048]{2,1,0:T(8,128)(2,1)S(1)}, bf16[1,256,2048]{2,1,0:T(8,128)(2,1)}, u32[]{:S(2)}) copy-start(bf16[1,256,2048]{2,1,0:T(8,128)(2,1)} %param.37) | copy-start | bytes 3145732
  7.2 143.3 %all-gather.9.cloned.1.call-start = ((), (), s32[]{:S(2)}) async-start(), calls=%async_computation.5 | async-start | bytes 5242880 | tf_op jit(solution)/shard_map/all_gather | solution.py:56
  13.5 64.2 %copy-start.1 = (bf16[512,256]{1,0:T(8,128)(2,1)S(1)}, bf16[512,256]{1,0:T(8,128)(2,1)}, u32[]{:S(2)}) copy-start(bf16[512,256]{1,0:T(8,128)(2,1)} %param.22) | copy-start | bytes 786436
  76.1 3.2 copy-start.5
  76.1 3.4 copy-start.3
  77.6 3.4 copy-start.2
  77.6 3.8 copy-start.6
  77.7 101.5 %all-gather.11.cloned.1.call-start = ((), (), s32[]{:S(2)}) async-start(), calls=%async_computation.6 | async-start | bytes 5242880 | tf_op jit(solution)/shard_map/all_gather | solution.py:56
  84.0 281.3 %reduce-scatter.5.cloned.1.call-start = ((), (), s32[]{:S(2)}) async-start(), calls=%async_computation.7 | async-start | bytes 10485760 | tf_op jit(solution)/shard_map/reduce_scatter | solution.py:251
  138.1 5.6 %copy-start.7 = (f32[256]{0:T(256)S(1)}, f32[256]{0:T(256)}, u32[]{:S(2)}) copy-start(f32[256]{0:T(256)} %param.27) | copy-start | bytes 3076
  179.2 3.9 copy-start.9
  179.2 4.1 copy-start.11
  179.2 4.4 copy-start.13
  183.6 2.2 copy-start.10
  295.8 67.1 %copy-start.4 = (bf16[8,64,2,128]{3,2,1,0:T(2,128)(2,1)S(1)}, bf16[8,64,2,128]{3,2,1,0:T(2,128)(2,1)}, u32[]{:S(2)}) copy-start(bf16[8,64,2,128]{3,2,1,0:T(2,128)(2,1)} %get-tuple-element.115) | copy-start | bytes 786436
  298.7 66.4 %copy-start.8 = (f32[256]{0:T(256)S(1)}, f32[256]{0:T(256)}, u32[]{:S(2)}) copy-start(f32[256]{0:T(256)} %param.29) | copy-start | bytes 3076
  365.3 65.8 %all-to-all-start.1 = ((bf16[64,8,2048]{2,1,0:T(8,128)(2,1)}), bf16[64,8,2048]{2,1,0:T(8,128)(2,1)S(1)}, u32[]{:S(2)}, u32[]{:S(2)}) async-start(bf16[64,8,2048]{2,1,0:T(8,128)(2,1)} %bitcast.561), calls=%async_computation.3 | async-start | bytes 4194304 | tf_op jit(solution)/shard_map/all_to_all | solution.py:259
  381.4 49.7 %copy-start.12 = (f32[128,2]{0,1:T(2,128)S(1)}, f32[128,2]{0,1:T(2,128)}, u32[]{:S(2)}) copy-start(f32[128,2]{0,1:T(2,128)} %param.34) | copy-start | bytes 3076
  381.4 51.3 %reduce-scatter.3.cloned.1.call-start = ((), (), s32[]{:S(2)}) async-start(), calls=%async_computation.4 | async-start | bytes 2621440 | tf_op jit(solution)/shard_map/reduce_scatter | solution.py:191
Sparse Core Ops, SparseCore 0:
  77.8 48.3 all-gather.8
  128.0 51.1 all-gather.10
  192.9 83.5 reduce-scatter.4
  385.0 31.9 reduce-scatter.2
where the time goes:
time: 443 us; the launch traced here: 439 us
  blocking collectives  185 us (42%)
  other arithmetic  85.1 us (19%)
  waiting for transfers between devices  70.4 us (16%)
  matrix products  47.9 us (11%)
  local copies, waits for them, and re-layouts  19.5 us (4%)
  starting transfers between devices  16.4 us (4%)
  between operations  14.3 us (3%)
    all_gather x12, blocking collectives, entering(): lax.all_gather(part.astype(kind), axis)  122 us
    all_to_all x1, blocking collectives, routed_half(): lax.all_to_all(outgoing.reshape(experts, slot_count, width_model), EP, sp...  62.6 us
    all_to_all x1, waiting for transfers between devices, routed_half(): lax.all_to_all(summed.reshape(experts, slot_count, width_model), EP, spli...  46.3 us
    reduce_sum x16, other arithmetic, advance(): jnp.sum(query_tile_rows[:, None] * address_piece_entries[None, :] * jnp.e...  31.5 us
    all_gather x2, waiting for transfers between devices, work_in_pieces(): outs.append(jax.vmap(apply)(lax.all_gather(share, axis), starts))  24 us
    all_to_all x1, starting transfers between devices, routed_half(): lax.all_to_all(summed.reshape(experts, slot_count, width_model), EP, spli...  16.1 us
    mul x16, other arithmetic, advance(): query_tile_rows * jnp.exp(progressive_summary)  15.5 us
    another operation x16, other arithmetic, advance(): progressive_summary = jnp.cumsum(decay_block, axis=0)  14.5 us
  transfers between devices with their start and end apart: 5, of which 2 were waited for; matrix products, arithmetic and copies ran while one was open for 30% of the time, Pallas kernels for 0%

commit v1 on v0

v1 whole, which is shorter than its diff:
```python
import functools

import jax
import jax.numpy as jnp
from jax import lax
from jax.experimental import pallas as pl
from jax.experimental.pallas import tpu as pltpu
from jax.sharding import Mesh
from jax.sharding import PartitionSpec as P

EP = ("ep_0", "ep_1", "ep_2")
EP_TP = ("ep_0", "ep_1", "ep_2", "tp")
EPS = 1e-06
TILE = 128
SUB = 16
CHUNKS = 4
MESH = pl.DeviceIdType.MESH
F32 = jnp.float32
BF16 = jnp.bfloat16


def dot_nt(a, b):
    return lax.dot_general(a, b, (((1,), (1,)), ((), ())), preferred_element_type=F32)


def dot_tn(a, b):
    return lax.dot_general(a, b, (((0,), (0,)), ((), ())), preferred_element_type=F32)


def dot(a, b):
    return jnp.dot(a, b, preferred_element_type=F32)


def sigmoid(x):
    return 1.0 / (1.0 + jnp.exp(-x))


def kernel(
    sizes,
    q_in,
    ff_in,
    fb_in,
    v_in,
    og_in,
    lbf_in,
    lbb_in,
    extra_in,
    hns_in,
    wo_in,
    res_in,
    ens_in,
    routes_in,
    mixw_in,
    g_in,
    u_in,
    d_in,
    mix_out,
    routed_out,
    q_v,
    ff_v,
    fb_v,
    v_v,
    og_v,
    lbf_v,
    lbb_v,
    extra_v,
    hns_v,
    wo_v,
    res_v,
    ens_v,
    routes_v,
    mixw_v,
    gu,
    dd,
    xn,
    pick,
    cwt,
    pk_send,
    arr,
    xs,
    hid,
    rt_send,
    rt_recv,
    p_s,
    k_s,
    qf,
    o_s,
    ust,
    tots,
    st_send,
    st_recv,
    inc_send,
    inc_recv,
    mh,
    mp_send,
    mp_recv,
    ld_sem,
    w_ssem,
    w_rsem,
    a_ssem,
    a_rsem,
    r_ssem,
    r_rsem,
    m_ssem,
    m_rsem,
):
    nz, nx, nc, nt = sizes
    count = nz * nx * nc
    rows = res_v.shape[0]
    width = res_v.shape[1]
    half = width // 2
    cap = pk_send.shape[1] // 2
    tokens = q_v.shape[0]
    tiles = tokens // TILE
    heads = q_v.shape[1] // TILE
    srows = st_send.shape[1] // 2
    per = TILE // srows
    ffp = gu.shape[-1]
    colc = width // CHUNKS
    halfc = colc // 2

    z, x, c = (lax.axis_index(a) for a in EP)
    t = lax.axis_index("tp")
    me = (z * nx + x) * nc + c

    def ep_id(p):
        return {
            "ep_0": lax.div(p, nx * nc),
            "ep_1": lax.rem(lax.div(p, nc), nx),
            "ep_2": lax.rem(p, nc),
            "tp": t,
        }

    def y_id(d):
        return {"ep_0": z, "ep_1": x, "ep_2": c, "tp": lax.rem(t + d, nt)}

    def peer_of(i):
        odd = lax.rem(i, 2)
        dist = odd * (count // 2 - lax.div(i + 1, 2)) - (1 - odd) * (count // 2 - lax.div(i, 2))
        return lax.rem(me + dist + count, count)

    t_rows = pl.ds(pl.multiple_of(t * rows, rows), rows)
    pairs = [
        (res_in.at[t_rows], res_v),
        (ens_in, ens_v),
        (routes_in, routes_v),
        (g_in.at[0], gu.at[0, 0]),
        (u_in.at[0], gu.at[0, 1]),
        (mixw_in, mixw_v),
        (q_in, q_v),
        (ff_in, ff_v),
        (fb_in, fb_v),
        (v_in, v_v),
        (og_in, og_v),
        (lbf_in, lbf_v),
        (lbb_in, lbb_v),
        (extra_in, extra_v),
        (hns_in, hns_v),
        (wo_in, wo_v),
    ] + [
        (d_in.at[0, :, j * colc : (j + 1) * colc], dd.at[j, 0 : d_in.shape[1]])
        for j in range(CHUNKS)
    ]
    loads = [pltpu.make_async_copy(a, b, ld_sem.at[i]) for i, (a, b) in enumerate(pairs)]
    for copy in loads:
        copy.start()

    barrier = pltpu.get_barrier_semaphore()

    @pl.loop(0, count - 1)
    def _(i):
        pl.semaphore_signal(barrier, inc=1, device_id=ep_id(peer_of(i)), device_id_type=MESH)

    for d in range(1, nt):
        pl.semaphore_signal(barrier, inc=1, device_id=y_id(d), device_id_type=MESH)

    for i in range(3):
        loads[i].wait()
    wide = res_v[...].astype(F32)
    scale = lax.rsqrt(jnp.mean(wide * wide, axis=-1, keepdims=True) + EPS)
    xn[...] = (wide * scale * ens_v[...]).astype(BF16)

    t_lanes = pl.ds(pl.multiple_of(t * rows, rows), rows)
    expert = lax.broadcasted_iota(jnp.int32, (count, rows), 0)
    hit0 = routes_v[0:1, t_lanes] == expert
    hit1 = routes_v[1:2, t_lanes] == expert
    member = jnp.where(hit0, 1.0, 0.0) + jnp.where(hit1, 1.0, 0.0)
    before = lax.broadcasted_iota(jnp.int32, (rows, rows), 0) < lax.broadcasted_iota(
        jnp.int32, (rows, rows), 1
    )
    rank = dot(member.astype(BF16), jnp.where(before, 1.0, 0.0).astype(BF16))
    slot = jnp.where(member > 0.5, rank, -1.0)
    seat = lax.broadcasted_iota(jnp.int32, (count, cap, rows), 1).astype(F32)
    chosen = jnp.where(jnp.abs(slot[:, None, :] - seat) < 0.25, 1.0, 0.0)
    pick[...] = chosen.reshape(count * cap, rows).astype(BF16)

    group = 64 // cap

    @pl.loop(0, count // group)
    def _(i):
        y = dot(pick[pl.ds(pl.multiple_of(i * 64, 64), 64), :], xn[...])
        lo = y[:, :half].reshape(group, cap, half)
        hi = y[:, half:].reshape(group, cap, half)
        pk_send[pl.ds(i * group, group)] = jnp.concatenate([lo, hi], axis=1).astype(BF16)

    for i in range(3, 5):
        loads[i].wait()
    pl.semaphore_wait(barrier, count - 1 + nt - 1)

    def y_copy(k, src, dst, d):
        return pltpu.make_async_remote_copy(
            src_ref=src,
            dst_ref=dst,
            send_sem=w_ssem.at[k],
            recv_sem=w_rsem.at[k],
            device_id=y_id(d),
            device_id_type=MESH,
        )

    g_up = y_copy(0, gu.at[0, 0], gu.at[1, 0], 1)
    u_up = y_copy(1, gu.at[0, 1], gu.at[1, 1], 1)
    u_dn = y_copy(2, gu.at[0, 1], gu.at[2, 1], nt - 1)
    g_dn = y_copy(3, gu.at[0, 0], gu.at[2, 0], nt - 1)
    g_far = y_copy(4, gu.at[1, 0], gu.at[3, 0], 1)
    u_far = y_copy(5, gu.at[2, 1], gu.at[3, 1], nt - 1)
    for copy in (g_up, u_dn, u_up, g_dn):
        copy.start()

    hh = ffp // 2

    def d_part(s, j, k):
        return dd.at[j, s * ffp + k * hh : s * ffp + (k + 1) * hh]

    def d_copies(j):
        base = 6 + 6 * j
        own = [y_copy(base + k, d_part(0, j, k), d_part(1, j, k), 1) for k in (0, 1)]
        own += [y_copy(base + 2 + k, d_part(0, j, k), d_part(2, j, k), nt - 1) for k in (1, 0)]
        far = [
            y_copy(base + 4, d_part(1, j, 0), d_part(3, j, 0), 1),
            y_copy(base + 5, d_part(2, j, 1), d_part(3, j, 1), nt - 1),
        ]
        return own, far

    d_all = [d_copies(j) for j in range(CHUNKS)]

    def exchange(src, dst, ssem, rsem):
        @pl.loop(0, count - 1)
        def _(i):
            p = peer_of(i)
            pltpu.make_async_remote_copy(
                src_ref=src.at[p],
                dst_ref=dst.at[me],
                send_sem=ssem,
                recv_sem=rsem,
                device_id=ep_id(p),
                device_id_type=MESH,
            ).start()

    def settle(ref, sem):
        part = ref.at[pl.ds(0, count - 1)]
        pltpu.make_async_copy(part, part, sem).wait()

    exchange(pk_send, arr, a_ssem.at[0], a_rsem.at[0])
    arr[me] = pk_send[me]

    for i in range(5, len(loads)):
        loads[i].wait()
    row_i = lax.broadcasted_iota(jnp.int32, (TILE, TILE), 0)
    col_i = lax.broadcasted_iota(jnp.int32, (TILE, TILE), 1)
    lower = row_i >= col_i
    upper = row_i <= col_i
    masks = (lower, upper)

    @pl.loop(0, tiles)
    def _(n):
        at = pl.ds(pl.multiple_of(n * TILE, TILE), TILE)
        for h in range(heads):
            ch = slice(h * TILE, (h + 1) * TILE)
            q = q_v[at, ch].astype(F32)
            qf[at, ch] = q * sigmoid(q)
            extra = jnp.broadcast_to(extra_v[h : h + 1, at], (TILE, TILE)).T
            for r, (f_ref, lb_ref) in enumerate(((ff_v, lbf_v), (fb_v, lbb_v))):
                key = sigmoid(-lb_ref[:, ch]) * sigmoid(-f_ref[at, ch].astype(F32))
                small = key * (
                    1.0
                    + key * (0.5 + key * ((1.0 / 3.0) + key * (0.25 + key * 0.2)))
                )
                near = key < 0.03125
                decay = jnp.where(near, -small, jnp.log(jnp.where(near, 0.5, 1.0 - key))) + extra
                tri = jnp.where(masks[r], 1.0, 0.0).astype(BF16)
                first = decay.astype(BF16)
                rest = decay - first.astype(F32)
                second = rest.astype(BF16)
                third = (rest - second.astype(F32)).astype(BF16)
                total = dot(tri, first) + (dot(tri, second) + dot(tri, third))
                p_s[r, at, ch] = total
                k_s[r, at, ch] = key
                last = total[TILE - 1 :, :] if r == 0 else total[:1, :]
                faded = (key * jnp.exp(last - total)).astype(BF16)
                ust[r * heads + h, n] = dot_tn(v_v[at, ch], faded)
                tots[r * heads + h, n] = jnp.broadcast_to(last, (8, TILE))

    for r in range(2):
        for h in range(heads):
            state = jnp.zeros((TILE, TILE), F32)
            log_total = jnp.zeros((1, TILE), F32)
            for n in range(tiles) if r == 0 else reversed(range(tiles)):
                row = tots[r * heads + h, n][:1]
                state = jnp.exp(row) * state + ust[r * heads + h, n]
                log_total = log_total + row
            message = jnp.concatenate(
                [
                    state.reshape(per, srows, TILE),
                    jnp.broadcast_to(log_total[None], (per, srows, TILE)),
                ],
                axis=1,
            )
            st_send[(r * heads + h) * per : (r * heads + h + 1) * per] = message.astype(BF16)

    exchange(st_send, st_recv, a_ssem.at[1], a_rsem.at[1])
    st_recv[me] = st_send[me]

    @pl.loop(0, tiles)
    def _(n):
        at = pl.ds(pl.multiple_of(n * TILE, TILE), TILE)
        for h in range(heads):
            ch = slice(h * TILE, (h + 1) * TILE)
            q = qf[at, ch]
            scores = None
            for r in range(2):
                total = p_s[r, at, ch]
                key = k_s[r, at, ch]
                blocks = []
                for i in range(TILE // SUB):
                    sub = slice(i * SUB, (i + 1) * SUB)
                    mid = total[i * SUB + SUB // 2 : i * SUB + SUB // 2 + 1, :]
                    q_i = (q[sub] * jnp.exp(total[sub] - mid)).astype(BF16)
                    k_i = (key * jnp.exp(jnp.minimum(mid - total, 70.0))).astype(BF16)
                    blocks.append(dot_nt(q_i, k_i))
                part = jnp.where(masks[r], jnp.concatenate(blocks, axis=0), 0.0)
                scores = part if scores is None else scores + part
            o_s[at, ch] = dot(scores.astype(BF16), v_v[at, ch])

    w0 = mixw_v[0:1, :]
    w1 = mixw_v[1:2, :]
    share = jnp.where(hit0, w0, 0.0) + jnp.where(hit1, w1, 0.0)
    weighted = chosen * share[:, None, :]
    blank = jnp.zeros_like(weighted)
    for k in range(2):
        both = jnp.concatenate([weighted, blank] if k == 0 else [blank, weighted], axis=1)
        flat = both.reshape(count * 2 * cap, rows).T
        high = flat.astype(BF16)
        cwt[0, k * rows : (k + 1) * rows] = high
        cwt[1, k * rows : (k + 1) * rows] = (flat - high.astype(F32)).astype(BF16)

    g_up.wait_recv()
    g_far.start()
    u_dn.wait_recv()
    u_far.start()
    for j in range(2):
        for copy in d_all[j][0]:
            copy.start()

    settle(arr, a_rsem.at[0])

    @pl.loop(0, count // group)
    def _(i):
        part = arr[pl.ds(i * group, group)].astype(F32)
        at = pl.ds(pl.multiple_of(i * 64, 64), 64)
        xs[at, :half] = part[:, :cap].reshape(64, half).astype(BF16)
        xs[at, half:] = part[:, cap:].reshape(64, half).astype(BF16)

    def lift(s):
        @pl.loop(0, count * cap // TILE)
        def _(i):
            at = pl.ds(pl.multiple_of(i * TILE, TILE), TILE)
            gated = dot(xs[at, :], gu[s, 0])
            lifted = dot(xs[at, :], gu[s, 1])
            hid[at, s * ffp : (s + 1) * ffp] = (gated * sigmoid(gated) * lifted).astype(BF16)

    lift(0)
    u_up.wait_recv()
    lift(1)
    g_dn.wait_recv()
    lift(2)

    settle(st_recv, a_rsem.at[1])
    side = lax.div(me * srows, heads * TILE)

    def pass_on(i, state):
        g = i + side * (count - 1 - 2 * i)
        inc_send[g] = state
        part = st_recv[g].astype(F32)
        return jnp.exp(part[srows:]) * state + part[:srows]

    lax.fori_loop(0, count, pass_on, jnp.zeros((srows, TILE), F32))
    exchange(inc_send, inc_recv, a_ssem.at[2], a_rsem.at[2])
    inc_recv[me] = inc_send[me]

    g_far.wait_recv()
    u_far.wait_recv()
    lift(3)

    def down(j):
        @pl.loop(0, count // group)
        def _(i):
            y = dot(hid[pl.ds(pl.multiple_of(i * 64, 64), 64), :], dd[j])
            lo = y[:, :halfc].reshape(group, cap, halfc)
            hi = y[:, halfc:].reshape(group, cap, halfc)
            rt_send[j, pl.ds(i * group, group)] = jnp.concatenate([lo, hi], axis=1).astype(BF16)

        exchange(rt_send.at[j], rt_recv.at[j], r_ssem.at[j], r_rsem.at[j])
        rt_recv[j, me] = rt_send[j, me]

    def finish_recurrence():
        settle(inc_recv, a_rsem.at[2])
        for r in range(2):
            for h in range(heads):
                ch = slice(h * TILE, (h + 1) * TILE)
                k = r * heads + h
                state = inc_recv[k * per : (k + 1) * per].reshape(TILE, TILE)
                for n in range(tiles) if r == 0 else reversed(range(tiles)):
                    at = slice(n * TILE, (n + 1) * TILE)
                    reach = (qf[at, ch] * jnp.exp(p_s[r, at, ch])).astype(BF16)
                    o_s[at, ch] += dot_nt(reach, state.astype(BF16))
                    state = jnp.exp(tots[k, n][:1]) * state + ust[k, n]

        @pl.loop(0, tiles)
        def _(n):
            at = pl.ds(pl.multiple_of(n * TILE, TILE), TILE)
            for h in range(heads):
                ch = slice(h * TILE, (h + 1) * TILE)
                o = o_s[at, ch]
                scaled = (
                    o
                    * lax.rsqrt(jnp.mean(o * o, axis=-1, keepdims=True) + EPS)
                    * hns_v[:, ch]
                )
                gate = og_v[at, ch].astype(F32)
                mh[at, ch] = (scaled * (gate * sigmoid(gate))).astype(BF16)

        @pl.loop(0, nt)
        def _(n):
            at = pl.ds(pl.multiple_of(n * rows, rows), rows)
            mp_send[n] = dot(mh[at, :], wo_v[...]).astype(BF16)

    for j in range(CHUNKS):
        own, far = d_all[j]
        own[0].wait_recv()
        far[0].start()
        own[2].wait_recv()
        far[1].start()
        if j + 2 < CHUNKS:
            for copy in d_all[j + 2][0]:
                copy.start()
        own[1].wait_recv()
        own[3].wait_recv()
        far[0].wait_recv()
        far[1].wait_recv()
        down(j)
        if j == 0:
            finish_recurrence()

    def mixer_copy(d):
        return pltpu.make_async_remote_copy(
            src_ref=mp_send.at[lax.rem(t + d, nt)],
            dst_ref=mp_recv.at[d - 1],
            send_sem=m_ssem.at[d - 1],
            recv_sem=m_rsem.at[d - 1],
            device_id=y_id(d),
            device_id_type=MESH,
        )

    mixers = [mixer_copy(d) for d in range(1, nt)]
    for copy in mixers:
        copy.start()

    def combine(j):
        settle(rt_recv.at[j], r_rsem.at[j])
        back = rt_recv[j].reshape(count * 2 * cap, halfc)
        y = dot(cwt[0], back) + dot(cwt[1], back)
        routed_out[:, j * colc : j * colc + halfc] = y[:rows].astype(BF16)
        routed_out[:, j * colc + halfc : (j + 1) * colc] = y[rows:].astype(BF16)

    for j in range(CHUNKS - 1):
        combine(j)
    for copy in mixers:
        copy.wait_recv()
    summed = mp_send[t].astype(F32)
    for d in range(nt - 1):
        summed = summed + mp_recv[d].astype(F32)
    mix_out[...] = summed.astype(BF16)
    combine(CHUNKS - 1)

    for copy in (g_up, u_up, u_dn, g_dn, g_far, u_far):
        copy.wait_send()
    for own, far in d_all:
        for copy in own + far:
            copy.wait_send()
    settle(pk_send, a_ssem.at[0])
    settle(st_send, a_ssem.at[1])
    settle(inc_send, a_ssem.at[2])
    for j in range(CHUNKS):
        settle(rt_send.at[j], r_ssem.at[j])
    for copy in mixers:
        copy.wait_send()


def shards(
    sizes,
    queries,
    forget_forward_logits,
    forget_backward_logits,
    values,
    output_gate_logits,
    lower_bound_forward,
    lower_bound_backward,
    extra_log_decay,
    head_norm_scale,
    output_projection,
    second_residual,
    expert_norm_scale,
    routes,
    specialist_mixing_factor,
    expert_gate_matrix,
    expert_up_matrix,
    expert_down_matrix,
):
    nz, nx, nc, nt = sizes
    count = nz * nx * nc
    tokens, width = second_residual.shape
    rows = tokens // nt
    cap = 4 * rows // count
    chan = queries.shape[1]
    heads = chan // TILE
    tiles = queries.shape[0] // TILE
    srows = 2 * heads * TILE // count
    ffp = expert_gate_matrix.shape[2]
    half = width // 2
    colc = width // CHUNKS
    operands = (
        queries,
        forget_forward_logits,
        forget_backward_logits,
        values,
        output_gate_logits,
        lower_bound_forward.reshape(1, chan),
        lower_bound_backward.reshape(1, chan),
        extra_log_decay.T,
        head_norm_scale.reshape(1, chan),
        output_projection,
        second_residual,
        expert_norm_scale.reshape(1, width),
        routes.T,
        specialist_mixing_factor.T,
        expert_gate_matrix,
        expert_up_matrix,
        expert_down_matrix,
    )
    vm = pltpu.VMEM
    scratch = [vm(a.shape, a.dtype) for a in operands[:10]]
    scratch += [vm((rows, width), BF16)]
    scratch += [vm(a.shape, a.dtype) for a in operands[11:14]]
    scratch += [
        vm((4, 2, width, ffp), BF16),
        vm((CHUNKS, 4 * ffp, colc), BF16),
        vm((rows, width), BF16),
        vm((count * cap, rows), BF16),
        vm((2, 2 * rows, count * 2 * cap), BF16),
        vm((count, 2 * cap, half), BF16),
        vm((count, 2 * cap, half), BF16),
        vm((count * cap, width), BF16),
        vm((count * cap, 4 * ffp), BF16),
        vm((CHUNKS, count, 2 * cap, colc // 2), BF16),
        vm((CHUNKS, count, 2 * cap, colc // 2), BF16),
        vm((2, tiles * TILE, chan), F32),
        vm((2, tiles * TILE, chan), F32),
        vm((tiles * TILE, chan), F32),
        vm((tiles * TILE, chan), F32),
        vm((2 * heads, tiles, TILE, TILE), F32),
        vm((2 * heads, tiles, 8, TILE), F32),
        vm((count, 2 * srows, TILE), BF16),
        vm((count, 2 * srows, TILE), BF16),
        vm((count, srows, TILE), F32),
        vm((count, srows, TILE), F32),
        vm((tiles * TILE, chan), BF16),
        vm((nt, rows, width), BF16),
        vm((nt - 1, rows, width), BF16),
        pltpu.SemaphoreType.DMA((16 + CHUNKS,)),
        pltpu.SemaphoreType.DMA((6 + 6 * CHUNKS,)),
        pltpu.SemaphoreType.DMA((6 + 6 * CHUNKS,)),
        pltpu.SemaphoreType.DMA((3,)),
        pltpu.SemaphoreType.DMA((3,)),
        pltpu.SemaphoreType.DMA((CHUNKS,)),
        pltpu.SemaphoreType.DMA((CHUNKS,)),
        pltpu.SemaphoreType.DMA((nt - 1,)),
        pltpu.SemaphoreType.DMA((nt - 1,)),
    ]
    out = jax.ShapeDtypeStruct((rows, width), BF16)
    return pl.pallas_call(
        functools.partial(kernel, sizes),
        out_shape=(out, out),
        in_specs=[pl.BlockSpec(memory_space=pl.ANY)] * len(operands),
        out_specs=(pl.BlockSpec(memory_space=pltpu.VMEM),) * 2,
        scratch_shapes=scratch,
        compiler_params=pltpu.CompilerParams(
            collective_id=0, has_side_effects=True, vmem_limit_bytes=62 * 1024 * 1024
        ),
    )(*operands)


def solution(mesh):
    tp = mesh.shape["tp"]
    ep = mesh.shape["ep"]
    sizes = (8, 4, 2, tp) if ep == 64 else (ep // 2, 1, 2, tp)
    split = Mesh(mesh.devices.reshape(sizes), EP_TP)
    return jax.shard_map(
        functools.partial(shards, sizes),
        mesh=split,
        in_specs=(
            P(EP, "tp"),
            P(EP, "tp"),
            P(EP, "tp"),
            P(EP, "tp"),
            P(EP, "tp"),
            P("tp"),
            P("tp"),
            P(EP, "tp"),
            P("tp"),
            P("tp", None),
            P(EP, None),
            P(),
            P(EP, None),
            P(EP_TP, None),
            P(EP, None, "tp"),
            P(EP, None, "tp"),
            P(EP, "tp", None),
        ),
        out_specs=(P(EP_TP, None), P(EP_TP, None)),
        check_vma=False,
    )
```

time: 443 us -> 158 us (0.36)
  blocking collectives: 185 us -> 0 us
  Pallas kernels: 0 us -> 152 us
  other arithmetic: 85.1 us -> 0 us
  waiting for transfers between devices: 70.4 us -> 0 us
  matrix products: 47.9 us -> 0 us
  starting transfers between devices: 16.4 us -> 0 us
  local copies, waits for them, and re-layouts: 19.5 us -> 3.76 us
  between operations: 14.3 us -> 0.65 us
    pallas_call x0 -> x1, Pallas kernels: none -> 152 us  [shards(): pl.pallas_call(functools.partial(kernel, sizes), out_shape=(out, out), in...]
    all_gather x12 -> x0, blocking collectives: 122 us -> none  [entering(): lax.all_gather(part.astype(kind), axis)]
    all_to_all x1 -> x0, blocking collectives: 62.6 us -> none  [routed_half(): lax.all_to_all(outgoing.reshape(experts, slot_count, width_model), EP, sp...]
    dot_general x58 -> x0, matrix products: 47.9 us -> none  [the longest x16 9.63 us: advance(): jnp.einsum('gkf,gkr->kfr', address_piece_entries * jnp.exp(segment_fading...]
    all_to_all x1 -> x0, waiting for transfers between devices: 46.3 us -> none  [routed_half(): lax.all_to_all(summed.reshape(experts, slot_count, width_model), EP, spli...]
    reduce_sum x19 -> x0, other arithmetic: 33 us -> none  [the longest x16 31.5 us: advance(): jnp.sum(query_tile_rows[:, None] * address_piece_entries[None, :] * jnp.e...]
    all_gather x2 -> x0, waiting for transfers between devices: 24 us -> none  [work_in_pieces(): outs.append(jax.vmap(apply)(lax.all_gather(share, axis), starts))]
    mul x22 -> x0, other arithmetic: 21.8 us -> none  [the longest x16 15.5 us: advance(): query_tile_rows * jnp.exp(progressive_summary)]
  transfers between devices with their start and end apart: 5 -> 0, of which waited for: 2 -> 0; matrix products, arithmetic and copies ran while one was open for 30% -> 0% of each run, Pallas kernels for 0% -> 0%
where the time goes in v1:
time: 158 us; the launch traced here: 156 us
  Pallas kernels  152 us (96%)
  local copies, waits for them, and re-layouts  3.76 us (2%)
    pallas_call x1, Pallas kernels, shards(): pl.pallas_call(functools.partial(kernel, sizes), out_shape=(out, out), in...  152 us
    unnamed x2, local copies, waits for them, and re-layouts  3.76 us

profile of v1, /device:TPU:1, one launch (start us, length us, event | category | flops | bytes accessed | tf_op | source)
XLA Modules:
  0.0 156.1 jit_solution(15343223570695998136)
XLA Ops:
  0.6 151.7 %shard_map.176 = (bf16[128,2048]{1,0:T(8,128)(2,1)}, bf16[128,2048]{1,0:T(8,128)(2,1)}) custom-call(bf16[512,256]{1,0:T(8,128)(2,1)} %q_in.1, bf16[512,256]{1,0:T(8,128)(2,1)} %ff_in.1, bf16[512,256]{1,0:T(8,128)(2,1)} %fb_in.1, bf16[512,256]{1,0:T(8,128)(2,1)} %v_in.1, bf16[512,256]{1,0:T(8,128)(2,1)} %og_in.1, f32[1,256]{1,0:T(1,128)} %bitcast.10, ...), custom_call_target="tpu_custom_call" | custom-call | tf_op jit(solution)/shard_map/pallas_call | solution.py:600
  152.3 1.9 %copy.21 = bf16[128,2048]{1,0:T(8,128)(2,1)} copy(bf16[128,2048]{1,0:T(8,128)(2,1)} %get-tuple-element.4) | data formatting | bytes 1048576
  154.2 1.9 %copy.22 = bf16[128,2048]{1,0:T(8,128)(2,1)} copy(bf16[128,2048]{1,0:T(8,128)(2,1)} %get-tuple-element.5) | data formatting | bytes 1048576

commit v2 on v1

--- a/solution.py
+++ b/solution.py
@@ -93,6 +93,7 @@
     inc_recv,
     mh,
     mp_send,
+    mp_sum,
     mp_recv,
     ld_sem,
     w_ssem,
@@ -103,6 +104,7 @@
     r_rsem,
     m_ssem,
     m_rsem,
+    d_rsem,
 ):
     nz, nx, nc, nt = sizes
     count = nz * nx * nc
@@ -134,18 +136,23 @@
     def y_id(d):
         return {"ep_0": z, "ep_1": x, "ep_2": c, "tp": lax.rem(t + d, nt)}
 
+    def reach(i):
+        odd = lax.rem(i, 2)
+        return odd * (count // 2 - lax.div(i + 1, 2)) - (1 - odd) * (count // 2 - lax.div(i, 2))
+
     def peer_of(i):
-        odd = lax.rem(i, 2)
-        dist = odd * (count // 2 - lax.div(i + 1, 2)) - (1 - odd) * (count // 2 - lax.div(i, 2))
-        return lax.rem(me + dist + count, count)
+        return lax.rem(me + reach(i) + count, count)
+
+    def source_of(i):
+        return lax.rem(me - reach(i) + count, count)
 
     t_rows = pl.ds(pl.multiple_of(t * rows, rows), rows)
     pairs = [
+        (g_in.at[0], gu.at[0, 0]),
+        (u_in.at[0], gu.at[0, 1]),
         (res_in.at[t_rows], res_v),
         (ens_in, ens_v),
         (routes_in, routes_v),
-        (g_in.at[0], gu.at[0, 0]),
-        (u_in.at[0], gu.at[0, 1]),
         (mixw_in, mixw_v),
         (q_in, q_v),
         (ff_in, ff_v),
@@ -157,7 +164,8 @@
         (extra_in, extra_v),
         (hns_in, hns_v),
         (wo_in, wo_v),
-    ] + [
+    ]
+    pairs[2:2] = [
         (d_in.at[0, :, j * colc : (j + 1) * colc], dd.at[j, 0 : d_in.shape[1]])
         for j in range(CHUNKS)
     ]
@@ -167,14 +175,57 @@
 
     barrier = pltpu.get_barrier_semaphore()
 
+    for d in range(1, nt):
+        pl.semaphore_signal(barrier, inc=1, device_id=y_id(d), device_id_type=MESH)
+
     @pl.loop(0, count - 1)
     def _(i):
         pl.semaphore_signal(barrier, inc=1, device_id=ep_id(peer_of(i)), device_id_type=MESH)
 
-    for d in range(1, nt):
-        pl.semaphore_signal(barrier, inc=1, device_id=y_id(d), device_id_type=MESH)
-
-    for i in range(3):
+    for i in range(2 + CHUNKS):
+        loads[i].wait()
+    pl.semaphore_wait(barrier, count - 1 + nt - 1)
+
+    def y_copy(k, src, dst, d):
+        return pltpu.make_async_remote_copy(
+            src_ref=src,
+            dst_ref=dst,
+            send_sem=w_ssem.at[k],
+            recv_sem=w_rsem.at[k],
+            device_id=y_id(d),
+            device_id_type=MESH,
+        )
+
+    g_up = y_copy(0, gu.at[0, 0], gu.at[1, 0], 1)
+    u_up = y_copy(1, gu.at[0, 1], gu.at[1, 1], 1)
+    u_dn = y_copy(2, gu.at[0, 1], gu.at[2, 1], nt - 1)
+    g_dn = y_copy(3, gu.at[0, 0], gu.at[2, 0], nt - 1)
+    g_far = y_copy(4, gu.at[1, 0], gu.at[3, 0], 1)
+    u_far = y_copy(5, gu.at[2, 1], gu.at[3, 1], nt - 1)
+    hh = ffp // 2
+
+    def d_part(s, j, k):
+        return dd.at[j, s * ffp + k * hh : s * ffp + (k + 1) * hh]
+
+    def d_copies(j):
+        base = 6 + 6 * j
+        own = [y_copy(base + k, d_part(0, j, k), d_part(1, j, k), 1) for k in (0, 1)]
+        own += [y_copy(base + 2 + k, d_part(0, j, k), d_part(2, j, k), nt - 1) for k in (1, 0)]
+        far = [
+            y_copy(base + 4, d_part(1, j, 0), d_part(3, j, 0), 1),
+            y_copy(base + 5, d_part(2, j, 1), d_part(3, j, 1), nt - 1),
+        ]
+        return own, far
+
+    d_all = [d_copies(j) for j in range(CHUNKS)]
+
+    for copy in (g_up, u_dn, u_up, g_dn):
+        copy.start()
+    for copy in d_all[0][0]:
+        copy.start()
+
+
+    for i in range(2 + CHUNKS, 5 + CHUNKS):
         loads[i].wait()
     wide = res_v[...].astype(F32)
     scale = lax.rsqrt(jnp.mean(wide * wide, axis=-1, keepdims=True) + EPS)
@@ -194,54 +245,15 @@
     chosen = jnp.where(jnp.abs(slot[:, None, :] - seat) < 0.25, 1.0, 0.0)
     pick[...] = chosen.reshape(count * cap, rows).astype(BF16)
 
-    group = 64 // cap
-
-    @pl.loop(0, count // group)
+    group = TILE // cap
+    parts = count // group
+
+    @pl.loop(0, parts)
     def _(i):
-        y = dot(pick[pl.ds(pl.multiple_of(i * 64, 64), 64), :], xn[...])
+        y = dot(pick[pl.ds(pl.multiple_of(i * TILE, TILE), TILE), :], xn[...])
         lo = y[:, :half].reshape(group, cap, half)
         hi = y[:, half:].reshape(group, cap, half)
         pk_send[pl.ds(i * group, group)] = jnp.concatenate([lo, hi], axis=1).astype(BF16)
-
-    for i in range(3, 5):
-        loads[i].wait()
-    pl.semaphore_wait(barrier, count - 1 + nt - 1)
-
-    def y_copy(k, src, dst, d):
-        return pltpu.make_async_remote_copy(
-            src_ref=src,
-            dst_ref=dst,
-            send_sem=w_ssem.at[k],
-            recv_sem=w_rsem.at[k],
-            device_id=y_id(d),
-            device_id_type=MESH,
-        )
-
-    g_up = y_copy(0, gu.at[0, 0], gu.at[1, 0], 1)
-    u_up = y_copy(1, gu.at[0, 1], gu.at[1, 1], 1)
-    u_dn = y_copy(2, gu.at[0, 1], gu.at[2, 1], nt - 1)
-    g_dn = y_copy(3, gu.at[0, 0], gu.at[2, 0], nt - 1)
-    g_far = y_copy(4, gu.at[1, 0], gu.at[3, 0], 1)
-    u_far = y_copy(5, gu.at[2, 1], gu.at[3, 1], nt - 1)
-    for copy in (g_up, u_dn, u_up, g_dn):
-        copy.start()
-
-    hh = ffp // 2
-
-    def d_part(s, j, k):
-        return dd.at[j, s * ffp + k * hh : s * ffp + (k + 1) * hh]
-
-    def d_copies(j):
-        base = 6 + 6 * j
-        own = [y_copy(base + k, d_part(0, j, k), d_part(1, j, k), 1) for k in (0, 1)]
-        own += [y_copy(base + 2 + k, d_part(0, j, k), d_part(2, j, k), nt - 1) for k in (1, 0)]
-        far = [
-            y_copy(base + 4, d_part(1, j, 0), d_part(3, j, 0), 1),
-            y_copy(base + 5, d_part(2, j, 1), d_part(3, j, 1), nt - 1),
-        ]
-        return own, far
-
-    d_all = [d_copies(j) for j in range(CHUNKS)]
 
     def exchange(src, dst, ssem, rsem):
         @pl.loop(0, count - 1)
@@ -260,10 +272,24 @@
         part = ref.at[pl.ds(0, count - 1)]
         pltpu.make_async_copy(part, part, sem).wait()
 
-    exchange(pk_send, arr, a_ssem.at[0], a_rsem.at[0])
-    arr[me] = pk_send[me]
-
-    for i in range(5, len(loads)):
+    def dispatch(k):
+        @pl.loop(k * group, min((k + 1) * group, count - 1))
+        def _(i):
+            p = peer_of(i)
+            pltpu.make_async_remote_copy(
+                src_ref=pk_send.at[p],
+                dst_ref=arr.at[i],
+                send_sem=a_ssem.at[0],
+                recv_sem=d_rsem.at[k],
+                device_id=ep_id(p),
+                device_id_type=MESH,
+            ).start()
+
+    for k in range(parts // 2):
+        dispatch(k)
+    arr[count - 1] = pk_send[me]
+
+    for i in range(5 + CHUNKS, len(loads)):
         loads[i].wait()
     row_i = lax.broadcasted_iota(jnp.int32, (TILE, TILE), 0)
     col_i = lax.broadcasted_iota(jnp.int32, (TILE, TILE), 1)
@@ -319,6 +345,8 @@
 
     exchange(st_send, st_recv, a_ssem.at[1], a_rsem.at[1])
     st_recv[me] = st_send[me]
+    for k in range(parts // 2, parts):
+        dispatch(k)
 
     @pl.loop(0, tiles)
     def _(n):
@@ -357,33 +385,6 @@
     g_far.start()
     u_dn.wait_recv()
     u_far.start()
-    for j in range(2):
-        for copy in d_all[j][0]:
-            copy.start()
-
-    settle(arr, a_rsem.at[0])
-
-    @pl.loop(0, count // group)
-    def _(i):
-        part = arr[pl.ds(i * group, group)].astype(F32)
-        at = pl.ds(pl.multiple_of(i * 64, 64), 64)
-        xs[at, :half] = part[:, :cap].reshape(64, half).astype(BF16)
-        xs[at, half:] = part[:, cap:].reshape(64, half).astype(BF16)
-
-    def lift(s):
-        @pl.loop(0, count * cap // TILE)
-        def _(i):
-            at = pl.ds(pl.multiple_of(i * TILE, TILE), TILE)
-            gated = dot(xs[at, :], gu[s, 0])
-            lifted = dot(xs[at, :], gu[s, 1])
-            hid[at, s * ffp : (s + 1) * ffp] = (gated * sigmoid(gated) * lifted).astype(BF16)
-
-    lift(0)
-    u_up.wait_recv()
-    lift(1)
-    g_dn.wait_recv()
-    lift(2)
-
     settle(st_recv, a_rsem.at[1])
     side = lax.div(me * srows, heads * TILE)
 
@@ -397,20 +398,36 @@
     exchange(inc_send, inc_recv, a_ssem.at[2], a_rsem.at[2])
     inc_recv[me] = inc_send[me]
 
-    g_far.wait_recv()
-    u_far.wait_recv()
-    lift(3)
-
-    def down(j):
-        @pl.loop(0, count // group)
+    def lift(s, lo, size):
+        at = pl.ds(pl.multiple_of(lo, TILE), size)
+        gated = dot(xs[at, :], gu[s, 0])
+        lifted = dot(xs[at, :], gu[s, 1])
+        hid[at, s * ffp : (s + 1) * ffp] = (gated * sigmoid(gated) * lifted).astype(BF16)
+
+    def lift_all(s):
+        @pl.loop(0, parts // 2)
         def _(i):
-            y = dot(hid[pl.ds(pl.multiple_of(i * 64, 64), 64), :], dd[j])
-            lo = y[:, :halfc].reshape(group, cap, halfc)
-            hi = y[:, halfc:].reshape(group, cap, halfc)
-            rt_send[j, pl.ds(i * group, group)] = jnp.concatenate([lo, hi], axis=1).astype(BF16)
-
-        exchange(rt_send.at[j], rt_recv.at[j], r_ssem.at[j], r_rsem.at[j])
-        rt_recv[j, me] = rt_send[j, me]
+            lift(s, i * (2 * TILE), 2 * TILE)
+
+    for k in range(parts):
+        landed = arr.at[pl.ds(0, min(group, count - 1 - k * group))]
+        pltpu.make_async_copy(landed, landed, d_rsem.at[k]).wait()
+        block = arr[k * group : (k + 1) * group].astype(F32)
+        at = slice(k * TILE, (k + 1) * TILE)
+        xs[at, :half] = block[:, :cap].reshape(TILE, half).astype(BF16)
+        xs[at, half:] = block[:, cap:].reshape(TILE, half).astype(BF16)
+        lift(0, k * TILE, TILE)
+
+    d_all[0][0][0].wait_recv()
+    d_all[0][1][0].start()
+    d_all[0][0][2].wait_recv()
+    d_all[0][1][1].start()
+    for copy in d_all[1][0]:
+        copy.start()
+    u_up.wait_recv()
+    lift_all(1)
+    g_dn.wait_recv()
+    lift_all(2)
 
     def finish_recurrence():
         settle(inc_recv, a_rsem.at[2])
@@ -444,36 +461,72 @@
             at = pl.ds(pl.multiple_of(n * rows, rows), rows)
             mp_send[n] = dot(mh[at, :], wo_v[...]).astype(BF16)
 
+    finish_recurrence()
+
+    g_far.wait_recv()
+    u_far.wait_recv()
+    lift_all(3)
+
+    def down(j):
+        @pl.loop(0, parts)
+        def _(i):
+            y = dot(hid[pl.ds(pl.multiple_of(i * TILE, TILE), TILE), :], dd[j])
+            lo = y[:, :halfc].reshape(group, cap, halfc)
+            hi = y[:, halfc:].reshape(group, cap, halfc)
+            rt_send[j, pl.ds(i * group, group)] = jnp.concatenate([lo, hi], axis=1).astype(BF16)
+
+        @pl.loop(0, count - 1)
+        def _(i):
+            p = source_of(i)
+            pltpu.make_async_remote_copy(
+                src_ref=rt_send.at[j, i],
+                dst_ref=rt_recv.at[j, me],
+                send_sem=r_ssem.at[j],
+                recv_sem=r_rsem.at[j],
+                device_id=ep_id(p),
+                device_id_type=MESH,
+            ).start()
+
+        rt_recv[j, me] = rt_send[j, count - 1]
+
+    hr = rows // 2
+
+    def mixer_copy(k, src, dst, d):
+        return pltpu.make_async_remote_copy(
+            src_ref=src,
+            dst_ref=mp_recv.at[dst],
+            send_sem=m_ssem.at[k],
+            recv_sem=m_rsem.at[k],
+            device_id=y_id(d),
+            device_id_type=MESH,
+        )
+
+    above, across, below = (lax.rem(t + d, nt) for d in (1, 2, 3))
+    mix_first = [
+        mixer_copy(0, mp_send.at[across, 0:hr], 0, 1),
+        mixer_copy(1, mp_send.at[across, hr:rows], 1, nt - 1),
+        mixer_copy(2, mp_send.at[above, hr:rows], 2, 1),
+        mixer_copy(3, mp_send.at[below, 0:hr], 3, nt - 1),
+    ]
+    mix_second = [
+        mixer_copy(4, mp_sum.at[0], 4, 1),
+        mixer_copy(5, mp_sum.at[1], 5, nt - 1),
+    ]
+
     for j in range(CHUNKS):
         own, far = d_all[j]
-        own[0].wait_recv()
-        far[0].start()
-        own[2].wait_recv()
-        far[1].start()
-        if j + 2 < CHUNKS:
-            for copy in d_all[j + 2][0]:
+        if j > 0:
+            own[0].wait_recv()
+            far[0].start()
+            own[2].wait_recv()
+            far[1].start()
+            for copy in d_all[j + 1][0] if j + 1 < CHUNKS else mix_first:
                 copy.start()
         own[1].wait_recv()
         own[3].wait_recv()
         far[0].wait_recv()
         far[1].wait_recv()
         down(j)
-        if j == 0:
-            finish_recurrence()
-
-    def mixer_copy(d):
-        return pltpu.make_async_remote_copy(
-            src_ref=mp_send.at[lax.rem(t + d, nt)],
-            dst_ref=mp_recv.at[d - 1],
-            send_sem=m_ssem.at[d - 1],
-            recv_sem=m_rsem.at[d - 1],
-            device_id=y_id(d),
-            device_id_type=MESH,
-        )
-
-    mixers = [mixer_copy(d) for d in range(1, nt)]
-    for copy in mixers:
-        copy.start()
 
     def combine(j):
         settle(rt_recv.at[j], r_rsem.at[j])
@@ -482,14 +535,20 @@
         routed_out[:, j * colc : j * colc + halfc] = y[:rows].astype(BF16)
         routed_out[:, j * colc + halfc : (j + 1) * colc] = y[rows:].astype(BF16)
 
+    mix_first[0].wait_recv()
+    mp_sum[0] = (mp_send[above, 0:hr].astype(F32) + mp_recv[0].astype(F32)).astype(BF16)
+    mix_second[0].start()
+    mix_first[1].wait_recv()
+    mp_sum[1] = (mp_send[below, hr:rows].astype(F32) + mp_recv[1].astype(F32)).astype(BF16)
+    mix_second[1].start()
     for j in range(CHUNKS - 1):
         combine(j)
-    for copy in mixers:
+    for copy in mix_first[2:] + mix_second:
         copy.wait_recv()
-    summed = mp_send[t].astype(F32)
-    for d in range(nt - 1):
-        summed = summed + mp_recv[d].astype(F32)
-    mix_out[...] = summed.astype(BF16)
+    for k, (one, two) in enumerate(((4, 3), (2, 5))):
+        at = slice(k * hr, (k + 1) * hr)
+        summed = mp_send[t, at].astype(F32) + mp_recv[one].astype(F32) + mp_recv[two].astype(F32)
+        mix_out[at, :] = summed.astype(BF16)
     combine(CHUNKS - 1)
 
     for copy in (g_up, u_up, u_dn, g_dn, g_far, u_far):
@@ -502,7 +561,7 @@
     settle(inc_send, a_ssem.at[2])
     for j in range(CHUNKS):
         settle(rt_send.at[j], r_ssem.at[j])
-    for copy in mixers:
+    for copy in mix_first + mix_second:
         copy.wait_send()
 
 
@@ -585,7 +644,8 @@
         vm((count, srows, TILE), F32),
         vm((tiles * TILE, chan), BF16),
         vm((nt, rows, width), BF16),
-        vm((nt - 1, rows, width), BF16),
+        vm((2, rows // 2, width), BF16),
+        vm((6, rows // 2, width), BF16),
         pltpu.SemaphoreType.DMA((16 + CHUNKS,)),
         pltpu.SemaphoreType.DMA((6 + 6 * CHUNKS,)),
         pltpu.SemaphoreType.DMA((6 + 6 * CHUNKS,)),
@@ -593,20 +653,21 @@
         pltpu.SemaphoreType.DMA((3,)),
         pltpu.SemaphoreType.DMA((CHUNKS,)),
         pltpu.SemaphoreType.DMA((CHUNKS,)),
-        pltpu.SemaphoreType.DMA((nt - 1,)),
-        pltpu.SemaphoreType.DMA((nt - 1,)),
+        pltpu.SemaphoreType.DMA((6,)),
+        pltpu.SemaphoreType.DMA((6,)),
+        pltpu.SemaphoreType.DMA((count * cap // TILE,)),
     ]
     out = jax.ShapeDtypeStruct((rows, width), BF16)
     return pl.pallas_call(
         functools.partial(kernel, sizes),
         out_shape=(out, out),
-        in_specs=[pl.BlockSpec(memory_space=pl.ANY)] * len(operands),
+        in_specs=[pl.BlockSpec(memory_space=pltpu.HBM)] * len(operands),
         out_specs=(pl.BlockSpec(memory_space=pltpu.VMEM),) * 2,
         scratch_shapes=scratch,
         compiler_params=pltpu.CompilerParams(
-            collective_id=0, has_side_effects=True, vmem_limit_bytes=62 * 1024 * 1024
+            collective_id=0, has_side_effects=True, vmem_limit_bytes=48 * 1024 * 1024
         ),
-    )(*operands)
+    )(*(pltpu.with_memory_space_constraint(a, pltpu.HBM) for a in operands))
 
 
 def solution(mesh):

time: 158 us -> 143 us (0.905); the launches traced: 156 us -> 143 us
  Pallas kernels: 152 us -> 141 us
  local copies, waits for them, and re-layouts: 3.76 us -> 1.59 us
    pallas_call x1, Pallas kernels: 152 us -> 141 us  [shards(): pl.pallas_call(functools.partial(kernel, sizes), out_shape=(out, out), in...]
    unnamed x2, local copies, waits for them, and re-layouts: 3.76 us -> 1.59 us
where the time goes in v2:
time: 143 us
  Pallas kernels  141 us (99%)
  local copies, waits for them, and re-layouts  1.59 us (1%)
    pallas_call x1, Pallas kernels, shards(): pl.pallas_call(functools.partial(kernel, sizes), out_shape=(out, out), in...  141 us

profile of v2, /device:TPU:1, one launch (start us, length us, event | category | flops | bytes accessed | tf_op | source)
XLA Modules:
  0.0 143.2 jit_solution(13135697877547352310)
XLA Ops:
  0.6 141.0 %shard_map.176 = (bf16[128,2048]{1,0:T(8,128)(2,1)S(1)}, bf16[128,2048]{1,0:T(8,128)(2,1)S(1)}) custom-call(bf16[512,256]{1,0:T(8,128)(2,1)} %q_in.1, bf16[512,256]{1,0:T(8,128)(2,1)} %ff_in.1, bf16[512,256]{1,0:T(8,128)(2,1)} %fb_in.1, bf16[512,256]{1,0:T(8,128)(2,1)} %v_in.1, bf16[512,256]{1,0:T(8,128)(2,1)} %og_in.1, f32[1,256]{1,0:T(1,128)} %bitcast.10, ...), custom_call_target="tpu_custom_call" | custom-call | tf_op jit(solution)/shard_map/pallas_call | solution.py:661
  141.6 0.8 copy.21
  142.4 0.8 copy.22

commit v3 on v2

--- a/solution.py
+++ b/solution.py
@@ -105,6 +105,7 @@
     m_ssem,
     m_rsem,
     d_rsem,
+    word_sem,
 ):
     nz, nx, nc, nt = sizes
     count = nz * nx * nc
@@ -173,18 +174,28 @@
     for copy in loads:
         copy.start()
 
+    def grid_id(dz=0, dx=0, dc=0, dy=0):
+        return {
+            "ep_0": lax.rem(z + dz, nz),
+            "ep_1": lax.rem(x + dx, nx),
+            "ep_2": lax.rem(c + dc, nc),
+            "tp": lax.rem(t + dy, nt),
+        }
+
+    def greet(sem, devices):
+        for device in devices:
+            pl.semaphore_signal(sem, inc=1, device_id=device, device_id_type=MESH)
+
+    line_y = [grid_id(dy=d) for d in range(1, nt)]
+    plane = [grid_id(dx=i, dc=j) for i in range(nx) for j in range(nc) if i + j > 0]
+    near_z = [grid_id(dz=d) for d in range(1, nz) if min(d, nz - d) <= (nz + 3) // 4]
+    near = line_y + plane + near_z
     barrier = pltpu.get_barrier_semaphore()
-
-    for d in range(1, nt):
-        pl.semaphore_signal(barrier, inc=1, device_id=y_id(d), device_id_type=MESH)
-
-    @pl.loop(0, count - 1)
-    def _(i):
-        pl.semaphore_signal(barrier, inc=1, device_id=ep_id(peer_of(i)), device_id_type=MESH)
+    greet(barrier, near)
 
     for i in range(2 + CHUNKS):
         loads[i].wait()
-    pl.semaphore_wait(barrier, count - 1 + nt - 1)
+    pl.semaphore_wait(barrier, len(near))
 
     def y_copy(k, src, dst, d):
         return pltpu.make_async_remote_copy(
@@ -223,6 +234,7 @@
         copy.start()
     for copy in d_all[0][0]:
         copy.start()
+    greet(word_sem.at[0], near_z)
 
 
     for i in range(2 + CHUNKS, 5 + CHUNKS):
@@ -230,6 +242,9 @@
     wide = res_v[...].astype(F32)
     scale = lax.rsqrt(jnp.mean(wide * wide, axis=-1, keepdims=True) + EPS)
     xn[...] = (wide * scale * ens_v[...]).astype(BF16)
+
+    pl.semaphore_wait(word_sem.at[0], len(near_z))
+    greet(word_sem.at[1], plane)
 
     t_lanes = pl.ds(pl.multiple_of(t * rows, rows), rows)
     expert = lax.broadcasted_iota(jnp.int32, (count, rows), 0)
@@ -271,6 +286,8 @@
     def settle(ref, sem):
         part = ref.at[pl.ds(0, count - 1)]
         pltpu.make_async_copy(part, part, sem).wait()
+
+    pl.semaphore_wait(word_sem.at[1], len(plane))
 
     def dispatch(k):
         @pl.loop(k * group, min((k + 1) * group, count - 1))
@@ -409,7 +426,7 @@
         def _(i):
             lift(s, i * (2 * TILE), 2 * TILE)
 
-    for k in range(parts):
+    def unpack(k):
         landed = arr.at[pl.ds(0, min(group, count - 1 - k * group))]
         pltpu.make_async_copy(landed, landed, d_rsem.at[k]).wait()
         block = arr[k * group : (k + 1) * group].astype(F32)
@@ -418,16 +435,27 @@
         xs[at, half:] = block[:, cap:].reshape(TILE, half).astype(BF16)
         lift(0, k * TILE, TILE)
 
+    for k in range(parts - 1):
+        unpack(k)
+    early = (parts - 1) * TILE
+    u_up.wait_recv()
+    g_dn.wait_recv()
+    for n in (1, 2):
+
+        @pl.loop(0, parts - 1)
+        def _(i):
+            lift(n, i * TILE, TILE)
+
+    unpack(parts - 1)
+    for n in (1, 2):
+        lift(n, early, TILE)
+
     d_all[0][0][0].wait_recv()
     d_all[0][1][0].start()
     d_all[0][0][2].wait_recv()
     d_all[0][1][1].start()
     for copy in d_all[1][0]:
         copy.start()
-    u_up.wait_recv()
-    lift_all(1)
-    g_dn.wait_recv()
-    lift_all(2)
 
     def finish_recurrence():
         settle(inc_recv, a_rsem.at[2])
@@ -468,25 +496,33 @@
     lift_all(3)
 
     def down(j):
-        @pl.loop(0, parts)
-        def _(i):
+        def product(i):
             y = dot(hid[pl.ds(pl.multiple_of(i * TILE, TILE), TILE), :], dd[j])
             lo = y[:, :halfc].reshape(group, cap, halfc)
             hi = y[:, halfc:].reshape(group, cap, halfc)
             rt_send[j, pl.ds(i * group, group)] = jnp.concatenate([lo, hi], axis=1).astype(BF16)
 
-        @pl.loop(0, count - 1)
-        def _(i):
-            p = source_of(i)
-            pltpu.make_async_remote_copy(
-                src_ref=rt_send.at[j, i],
-                dst_ref=rt_recv.at[j, me],
-                send_sem=r_ssem.at[j],
-                recv_sem=r_rsem.at[j],
-                device_id=ep_id(p),
-                device_id_type=MESH,
-            ).start()
-
+        def give_back(first, last):
+            @pl.loop(first, last)
+            def _(i):
+                p = source_of(i)
+                pltpu.make_async_remote_copy(
+                    src_ref=rt_send.at[j, i],
+                    dst_ref=rt_recv.at[j, me],
+                    send_sem=r_ssem.at[j],
+                    recv_sem=r_rsem.at[j],
+                    device_id=ep_id(p),
+                    device_id_type=MESH,
+                ).start()
+
+        product(0)
+
+        @pl.loop(1, parts)
+        def _(k):
+            product(k)
+            give_back((k - 1) * group, k * group)
+
+        give_back((parts - 1) * group, count - 1)
         rt_recv[j, me] = rt_send[j, count - 1]
 
     hr = rows // 2
@@ -656,6 +692,7 @@
         pltpu.SemaphoreType.DMA((6,)),
         pltpu.SemaphoreType.DMA((6,)),
         pltpu.SemaphoreType.DMA((count * cap // TILE,)),
+        pltpu.SemaphoreType.REGULAR((2,)),
     ]
     out = jax.ShapeDtypeStruct((rows, width), BF16)
     return pl.pallas_call(

time: 143 us -> 141 us (0.986)
  Pallas kernels: 141 us -> 139 us
    pallas_call x1, Pallas kernels: 141 us -> 139 us  [shards(): pl.pallas_call(functools.partial(kernel, sizes), out_shape=(out, out), in...]
where the time goes in v3:
time: 141 us
  Pallas kernels  139 us (99%)
  local copies, waits for them, and re-layouts  1.59 us (1%)
    pallas_call x1, Pallas kernels, shards(): pl.pallas_call(functools.partial(kernel, sizes), out_shape=(out, out), in...  139 us

profile of v3, /device:TPU:1, one launch (start us, length us, event | category | flops | bytes accessed | tf_op | source)
XLA Modules:
  0.0 140.8 jit_solution(6392117294987839166)
XLA Ops:
  0.6 138.6 %shard_map.176 = (bf16[128,2048]{1,0:T(8,128)(2,1)S(1)}, bf16[128,2048]{1,0:T(8,128)(2,1)S(1)}) custom-call(bf16[512,256]{1,0:T(8,128)(2,1)} %q_in.1, bf16[512,256]{1,0:T(8,128)(2,1)} %ff_in.1, bf16[512,256]{1,0:T(8,128)(2,1)} %fb_in.1, bf16[512,256]{1,0:T(8,128)(2,1)} %v_in.1, bf16[512,256]{1,0:T(8,128)(2,1)} %og_in.1, f32[1,256]{1,0:T(1,128)} %bitcast.10, ...), custom_call_target="tpu_custom_call" | custom-call | tf_op jit(solution)/shard_map/pallas_call | solution.py:698
  139.2 0.8 copy.21
  140.0 0.8 copy.22

commit v4 on v3

--- a/solution.py
+++ b/solution.py
@@ -13,7 +13,8 @@
 EPS = 1e-06
 TILE = 128
 SUB = 16
-CHUNKS = 4
+EIGHTHS = (1, 2, 2, 3)
+CHUNKS = len(EIGHTHS)
 MESH = pl.DeviceIdType.MESH
 F32 = jnp.float32
 BF16 = jnp.bfloat16
@@ -71,7 +72,10 @@
     routes_v,
     mixw_v,
     gu,
-    dd,
+    dd0,
+    dd1,
+    dd2,
+    dd3,
     xn,
     pick,
     cwt,
@@ -79,8 +83,14 @@
     arr,
     xs,
     hid,
-    rt_send,
-    rt_recv,
+    rts0,
+    rts1,
+    rts2,
+    rts3,
+    rtr0,
+    rtr1,
+    rtr2,
+    rtr3,
     p_s,
     k_s,
     qf,
@@ -119,8 +129,11 @@
     srows = st_send.shape[1] // 2
     per = TILE // srows
     ffp = gu.shape[-1]
-    colc = width // CHUNKS
-    halfc = colc // 2
+    dd = (dd0, dd1, dd2, dd3)
+    rt_send = (rts0, rts1, rts2, rts3)
+    rt_recv = (rtr0, rtr1, rtr2, rtr3)
+    cols = [width * n // 8 for n in EIGHTHS]
+    starts = [sum(cols[:j]) for j in range(CHUNKS)]
 
     z, x, c = (lax.axis_index(a) for a in EP)
     t = lax.axis_index("tp")
@@ -167,7 +180,7 @@
         (wo_in, wo_v),
     ]
     pairs[2:2] = [
-        (d_in.at[0, :, j * colc : (j + 1) * colc], dd.at[j, 0 : d_in.shape[1]])
+        (d_in.at[0, :, starts[j] : starts[j] + cols[j]], dd[j].at[0:ffp])
         for j in range(CHUNKS)
     ]
     loads = [pltpu.make_async_copy(a, b, ld_sem.at[i]) for i, (a, b) in enumerate(pairs)]
@@ -216,7 +229,7 @@
     hh = ffp // 2
 
     def d_part(s, j, k):
-        return dd.at[j, s * ffp + k * hh : s * ffp + (k + 1) * hh]
+        return dd[j].at[s * ffp + k * hh : s * ffp + (k + 1) * hh]
 
     def d_copies(j):
         base = 6 + 6 * j
@@ -496,19 +509,21 @@
     lift_all(3)
 
     def down(j):
+        halfc = cols[j] // 2
+
         def product(i):
-            y = dot(hid[pl.ds(pl.multiple_of(i * TILE, TILE), TILE), :], dd[j])
+            y = dot(hid[pl.ds(pl.multiple_of(i * TILE, TILE), TILE), :], dd[j][...])
             lo = y[:, :halfc].reshape(group, cap, halfc)
             hi = y[:, halfc:].reshape(group, cap, halfc)
-            rt_send[j, pl.ds(i * group, group)] = jnp.concatenate([lo, hi], axis=1).astype(BF16)
+            rt_send[j][pl.ds(i * group, group)] = jnp.concatenate([lo, hi], axis=1).astype(BF16)
 
         def give_back(first, last):
             @pl.loop(first, last)
             def _(i):
                 p = source_of(i)
                 pltpu.make_async_remote_copy(
-                    src_ref=rt_send.at[j, i],
-                    dst_ref=rt_recv.at[j, me],
+                    src_ref=rt_send[j].at[i],
+                    dst_ref=rt_recv[j].at[me],
                     send_sem=r_ssem.at[j],
                     recv_sem=r_rsem.at[j],
                     device_id=ep_id(p),
@@ -523,7 +538,7 @@
             give_back((k - 1) * group, k * group)
 
         give_back((parts - 1) * group, count - 1)
-        rt_recv[j, me] = rt_send[j, count - 1]
+        rt_recv[j][me] = rt_send[j][count - 1]
 
     hr = rows // 2
 
@@ -565,11 +580,12 @@
         down(j)
 
     def combine(j):
-        settle(rt_recv.at[j], r_rsem.at[j])
-        back = rt_recv[j].reshape(count * 2 * cap, halfc)
+        settle(rt_recv[j], r_rsem.at[j])
+        halfc = cols[j] // 2
+        back = rt_recv[j][...].reshape(count * 2 * cap, halfc)
         y = dot(cwt[0], back) + dot(cwt[1], back)
-        routed_out[:, j * colc : j * colc + halfc] = y[:rows].astype(BF16)
-        routed_out[:, j * colc + halfc : (j + 1) * colc] = y[rows:].astype(BF16)
+        routed_out[:, starts[j] : starts[j] + halfc] = y[:rows].astype(BF16)
+        routed_out[:, starts[j] + halfc : starts[j] + cols[j]] = y[rows:].astype(BF16)
 
     mix_first[0].wait_recv()
     mp_sum[0] = (mp_send[above, 0:hr].astype(F32) + mp_recv[0].astype(F32)).astype(BF16)
@@ -596,7 +612,7 @@
     settle(st_send, a_ssem.at[1])
     settle(inc_send, a_ssem.at[2])
     for j in range(CHUNKS):
-        settle(rt_send.at[j], r_ssem.at[j])
+        settle(rt_send[j], r_ssem.at[j])
     for copy in mix_first + mix_second:
         copy.wait_send()
 
@@ -632,7 +648,7 @@
     srows = 2 * heads * TILE // count
     ffp = expert_gate_matrix.shape[2]
     half = width // 2
-    colc = width // CHUNKS
+    cols = [width * n // 8 for n in EIGHTHS]
     operands = (
         queries,
         forget_forward_logits,
@@ -658,7 +674,9 @@
     scratch += [vm(a.shape, a.dtype) for a in operands[11:14]]
     scratch += [
         vm((4, 2, width, ffp), BF16),
-        vm((CHUNKS, 4 * ffp, colc), BF16),
+    ]
+    scratch += [vm((4 * ffp, n), BF16) for n in cols]
+    scratch += [
         vm((rows, width), BF16),
         vm((count * cap, rows), BF16),
         vm((2, 2 * rows, count * 2 * cap), BF16),
@@ -666,8 +684,9 @@
         vm((count, 2 * cap, half), BF16),
         vm((count * cap, width), BF16),
         vm((count * cap, 4 * ffp), BF16),
-        vm((CHUNKS, count, 2 * cap, colc // 2), BF16),
-        vm((CHUNKS, count, 2 * cap, colc // 2), BF16),
+    ]
+    scratch += [vm((count, 2 * cap, n // 2), BF16) for n in cols + cols]
+    scratch += [
         vm((2, tiles * TILE, chan), F32),
         vm((2, tiles * TILE, chan), F32),
         vm((tiles * TILE, chan), F32),

time: 141 us -> 139 us (0.986)
  Pallas kernels: 139 us -> 137 us
    pallas_call x1, Pallas kernels: 139 us -> 137 us  [shards(): pl.pallas_call(functools.partial(kernel, sizes), out_shape=(out, out), in...]
where the time goes in v4:
time: 139 us
  Pallas kernels  137 us (99%)
  local copies, waits for them, and re-layouts  1.59 us (1%)
    pallas_call x1, Pallas kernels, shards(): pl.pallas_call(functools.partial(kernel, sizes), out_shape=(out, out), in...  137 us

profile of v4, /device:TPU:1, one launch (start us, length us, event | category | flops | bytes accessed | tf_op | source)
XLA Modules:
  0.0 138.9 jit_solution(14919019989435982164)
XLA Ops:
  0.6 136.6 %shard_map.176 = (bf16[128,2048]{1,0:T(8,128)(2,1)S(1)}, bf16[128,2048]{1,0:T(8,128)(2,1)S(1)}) custom-call(bf16[512,256]{1,0:T(8,128)(2,1)} %q_in.1, bf16[512,256]{1,0:T(8,128)(2,1)} %ff_in.1, bf16[512,256]{1,0:T(8,128)(2,1)} %fb_in.1, bf16[512,256]{1,0:T(8,128)(2,1)} %v_in.1, bf16[512,256]{1,0:T(8,128)(2,1)} %og_in.1, f32[1,256]{1,0:T(1,128)} %bitcast.10, ...), custom_call_target="tpu_custom_call" | custom-call | tf_op jit(solution)/shard_map/pallas_call | solution.py:717
  137.3 0.8 copy.21
  138.1 0.8 copy.22
